TPU v7x, 32 devices: a whole 2x2x4 slice. The times are simulated.
32 devices in a mesh: grp: 2 (over y), fs: 4 (over z), tp: 4 (over x, core).
Axes of the slice: x: 2, y: 2, z: 4, core: 2. Of those that a mesh axis runs over, the one named last changes fastest.
Arguments:
- tokens: bfloat16 [8, 384, 2048], P(('grp', 'fs'), None, 'tp'), parts along dimension 0, may hold values from -16 to 16
- norm_gain: float32 [2048], P('tp'), may hold values from 0.1 to 1.9
- in_weight: bfloat16 [2048, 1024], P('fs', 'tp'), may hold values from -0.125 to 0.125
- pool_weight: bfloat16 [8, 128, 128], P('tp'), may hold values from -0.5 to 0.5
- pool_scale: float32 [1024], P('tp'), may hold values from 0.1 to 1.9
- out_weight: bfloat16 [1024, 2048], P('fs', 'tp'), may hold values from -0.1875 to 0.1875
- ffn_gain: float32 [2048], P('tp'), may hold values from 0.1 to 1.9
- gate_weight: bfloat16 [2048, 5632], P('fs', 'tp'), may hold values from -0.125 to 0.125
- up_weight: bfloat16 [2048, 5632], P('fs', 'tp'), may hold values from -0.125 to 0.125
- down_weight: bfloat16 [5632, 2048], P('tp', 'fs'), may hold values from -0.078125 to 0.078125
Outputs:
- output: bfloat16 [8, 384, 2048], P(('grp', 'fs'), None, 'tp'), parts along dimension 0
There are 2 independent parts, one for each index of `grp`. A program takes and returns all parts, laid end to end along the dimension named above; an argument that names none is the same for every part. Nothing has to cross between parts.
All inputs are finite; a program needn't handle non-finite values.
Results may differ from a plain program's by a relative error of at most 0.009.
Values may be sent and summed in bfloat16 or wider, within the bound.
A program may use at most 64 MiB of HBM per device.

v0:
```python
import jax
import jax.numpy as jnp
from jax import lax
from jax.sharding import PartitionSpec as P

D = 2048
GD = 128
EPSILON = 0.05
HALVES = (1, 2, 4, 8)


def local(
    tokens,
    norm_gain,
    in_weight,
    pool_weight,
    pool_scale,
    out_weight,
    ffn_gain,
    gate_weight,
    up_weight,
    down_weight,
):
    seq_local, length, feat_local = tokens.shape
    stream = tokens.astype(jnp.float32)
    first_square = lax.psum(jnp.sum(stream * stream, axis=-1), "tp")
    normed = (stream * lax.rsqrt(first_square[..., None] / D + EPSILON) * norm_gain).astype(
        jnp.bfloat16
    )
    in_full = lax.all_gather(in_weight, "fs", axis=0, tiled=True)
    channels = in_full.shape[1]
    weight_rows = in_full
    pool_input = jnp.einsum(
        "slk,kc->slc",
        lax.all_gather(normed, "tp", axis=2, tiled=True),
        weight_rows,
        preferred_element_type=jnp.float32,
    ).astype(jnp.bfloat16)
    pool_float = pool_input.astype(jnp.float32)
    group_local = pool_weight.shape[0]
    group_ids = lax.axis_index("tp") * group_local + jnp.arange(channels) // GD
    selector = group_ids % 4
    running = jnp.concatenate(
        [jnp.zeros((seq_local, 1, channels), jnp.float32), jnp.cumsum(pool_float, axis=1)], axis=1
    )
    position = jnp.arange(length)
    window_mean = jnp.zeros_like(pool_float)
    for window_index, half_width in enumerate(HALVES):
        upper_sum = jnp.concatenate(
            [running[:, half_width:], jnp.repeat(running[:, -1:], half_width, axis=1)], axis=1
        )[:, :length]
        lower_sum = jnp.concatenate(
            [
                jnp.zeros((seq_local, half_width, channels), jnp.float32),
                running[:, : length + 1 - half_width],
            ],
            axis=1,
        )[:, :length]
        counts = (
            jnp.minimum(position + half_width, length) - jnp.maximum(position - half_width, 0)
        ).astype(jnp.float32)
        window_mean = jnp.where(
            selector == window_index, (upper_sum - lower_sum) / counts[:, None], window_mean
        )
    deviation = (window_mean - pool_float).astype(jnp.bfloat16)
    grouped = deviation.reshape(seq_local, length, group_local, GD)
    mapped = jnp.einsum("slgc,gcd->slgd", grouped, pool_weight, preferred_element_type=jnp.float32)
    pooled = (mapped.reshape(seq_local, length, channels) * pool_scale).astype(jnp.bfloat16)
    out_full = lax.all_gather(out_weight, "fs", axis=0, tiled=True)
    weight_rows = out_full
    mixed = stream + jnp.einsum(
        "jut,tx->jux",
        lax.all_gather(pooled, "tp", axis=2, tiled=True),
        weight_rows,
        preferred_element_type=jnp.float32,
    )
    second_square = lax.psum(jnp.sum(mixed * mixed, axis=-1), "tp")
    normed_two = (mixed * lax.rsqrt(second_square[..., None] / D + EPSILON) * ffn_gain).astype(
        jnp.bfloat16
    )
    features_full = lax.all_gather(normed_two, "tp", axis=2, tiled=True)
    gate_sum = jnp.einsum(
        "slk,kf->slf",
        features_full,
        lax.all_gather(gate_weight, "fs", axis=0, tiled=True),
        preferred_element_type=jnp.float32,
    )
    up_sum = jnp.einsum(
        "slk,kf->slf",
        features_full,
        lax.all_gather(up_weight, "fs", axis=0, tiled=True),
        preferred_element_type=jnp.float32,
    )
    hidden = (jax.nn.silu(gate_sum) * up_sum).astype(jnp.bfloat16)
    partial_value = jnp.einsum(
        "hor,rn->hon",
        hidden,
        lax.all_gather(down_weight, "fs", axis=1, tiled=True),
        preferred_element_type=jnp.float32,
    )
    summed = lax.psum_scatter(
        partial_value.astype(jnp.bfloat16), "tp", scatter_dimension=2, tiled=True
    ).astype(jnp.float32)
    return (mixed + summed).astype(jnp.bfloat16)


def solution(mesh):
    return jax.shard_map(
        local,
        mesh=mesh,
        in_specs=(
            P(("grp", "fs"), None, "tp"),
            P("tp"),
            P("fs", "tp"),
            P("tp", None, None),
            P("tp"),
            P("fs", "tp"),
            P("tp"),
            P("fs", "tp"),
            P("fs", "tp"),
            P("tp", "fs"),
        ),
        out_specs=P(("grp", "fs"), None, "tp"),
        check_vma=False,
    )
```

profile of v0, /device:TPU:0, one launch (start us, length us, event | category | flops | bytes accessed | tf_op | source)
XLA Modules:
  0.0 485.2 jit_solution(12671679941246397171)
XLA Ops:
  6.5 0.7 all-gather.10.cloned.1.call-update
  7.3 1.2 fusion.17
  8.5 8.4 %psum.14 = f32[1,384]{1,0:T(1,128)S(1)} all-reduce(f32[1,384]{1,0:T(1,128)S(1)} %reduce_sum.23), channel_id=1, replica_groups=mesh['grp'=2,'fs'=4,'tp'=4] {'tp'}, use_global_device_ids=true, to_apply=%region_1.0 | all-reduce | flops 384 | bytes 3072 | tf_op jit(solution)/shard_map/psum | solution.py:26
  16.9 1.9 fusion.19
  18.8 0.7 all-gather.12.cloned.1.call-update
  19.6 20.0 %all-gather.10.cloned.1.call-done = bf16[2048,256]{1,0:T(8,128)(2,1)} async-done(((bf16[512,256]{1,0:T(8,128)(2,1)}), bf16[2048,256]{1,0:T(8,128)(2,1)}) %all-gather.10.cloned.1.call-update) | async-done | bytes 1048592 | tf_op jit(solution)/shard_map/all_gather | solution.py:30
  39.6 20.6 %all-gather.8.cloned.1.call-done = bf16[1,384,2048]{2,1,0:T(8,128)(2,1)} async-done(((bf16[1,384,512]{2,1,0:T(8,128)(2,1)}), bf16[1,384,2048]{2,1,0:T(8,128)(2,1)}) %all-gather.8.cloned.1.call-update) | async-done | bytes 1572880 | tf_op jit(solution)/shard_map/all_gather | solution.py:35
  60.2 2.3 fusion.14
  62.5 0.3 fusion.23
  62.8 0.1 copy.12
  63.0 0.1 fusion.63
  63.1 0.1 fusion.61
  63.1 0.1 fusion.62
  63.3 0.5 fusion.39
  63.8 0.3 fusion.40
  64.1 0.1 fusion.38
  64.2 8.6 %all_gather.26 = bf16[1,384,1024]{1,2,0:T(8,128)(2,1)S(1)} all-gather(bf16[1,384,256]{1,2,0:T(8,128)(2,1)S(1)} %fusion.38), channel_id=1, replica_groups=mesh['grp'=2,'fs'=4,'tp'=4] {'tp'}, dimensions={2}, use_global_device_ids=true | all-gather | bytes 983040 | tf_op jit(solution)/shard_map/all_gather | solution.py:73
  72.8 17.0 %all-gather.12.cloned.1.call-done = bf16[1024,512]{1,0:T(8,128)(2,1)} async-done(((bf16[256,512]{1,0:T(8,128)(2,1)}), bf16[1024,512]{1,0:T(8,128)(2,1)}) %all-gather.12.cloned.1.call-update) | async-done | bytes 1048592 | tf_op jit(solution)/shard_map/all_gather | solution.py:69
  89.8 1.9 multiply_reduce_fusion
  91.8 6.1 %psum.15 = f32[1,384]{1,0:T(1,128)S(1)} all-reduce(f32[1,384]{1,0:T(1,128)S(1)} %reduce_sum.25), channel_id=1, replica_groups=mesh['grp'=2,'fs'=4,'tp'=4] {'tp'}, use_global_device_ids=true, to_apply=%region_5.6 | all-reduce | flops 384 | bytes 3072 | tf_op jit(solution)/shard_map/psum | solution.py:77
  97.9 0.9 multiply_convert_fusion
  98.8 0.5 all-gather.16.cloned.1.call-update
  99.4 0.5 all-gather.18.cloned.1.call-update
  100.0 0.7 all-gather.20.cloned.1.call-update
  100.7 17.0 %all-gather.14.cloned.1.call-done = bf16[1,384,2048]{2,1,0:T(8,128)(2,1)} async-done(((bf16[1,384,512]{2,1,0:T(8,128)(2,1)}), bf16[1,384,2048]{2,1,0:T(8,128)(2,1)}) %all-gather.14.cloned.1.call-update) | async-done | bytes 1572880 | tf_op jit(solution)/shard_map/all_gather | solution.py:81
  117.8 108.1 %all-gather.16.cloned.1.call-done = bf16[2048,1408]{1,0:T(8,128)(2,1)} async-done(((bf16[512,1408]{1,0:T(8,128)(2,1)}), bf16[2048,1408]{1,0:T(8,128)(2,1)}) %all-gather.16.cloned.1.call-update) | async-done | bytes 5767184 | tf_op jit(solution)/shard_map/all_gather | solution.py:85
  225.9 7.1 %fusion.3 = f32[384,1408]{1,0:T(8,128)} fusion(bf16[2048,1408]{1,0:T(8,128)(2,1)} %all-gather.16.cloned.1.call-done, bf16[1,384,2048]{2,1,0:T(8,128)(2,1)} %all-gather.14.cloned.1.call-done), kind=kOutput, calls=%fused_computation.5 | convolution fusion | flops 2214592512 | bytes 9502720 | tf_op jit(solution)/shard_map/slk,kf->slf/dot_general | solution.py:82
  233.0 99.3 %all-gather.18.cloned.1.call-done = bf16[2048,1408]{1,0:T(8,128)(2,1)} async-done(((bf16[512,1408]{1,0:T(8,128)(2,1)}), bf16[2048,1408]{1,0:T(8,128)(2,1)}) %all-gather.18.cloned.1.call-update) | async-done | bytes 5767184 | tf_op jit(solution)/shard_map/all_gather | solution.py:91
  332.3 106.5 %all-gather.20.cloned.1.call-done = bf16[1408,2048]{1,0:T(8,128)(2,1)} async-done(((bf16[1408,512]{1,0:T(8,128)(2,1)}), bf16[1408,2048]{1,0:T(8,128)(2,1)}) %all-gather.20.cloned.1.call-update) | async-done | bytes 5767184 | tf_op jit(solution)/shard_map/all_gather | solution.py:98
  438.9 11.3 %fusion.1 = bf16[1,384,2048]{2,1,0:T(8,128)(2,1)} fusion(bf16[1408,2048]{1,0:T(8,128)(2,1)} %all-gather.20.cloned.1.call-done, bf16[2048,1408]{1,0:T(8,128)(2,1)} %all-gather.18.cloned.1.call-done, f32[384,1408]{1,0:T(8,128)} %fusion.3, bf16[1,384,2048]{2,1,0:T(8,128)(2,1)S(1)} %copy-done.4), kind=kOutput, calls=%fused_computation.3 | convolution fusion | flops 4433215488 | bytes 16842752 | tf_op jit(solution)/shard_map/hor,rn->hon/dot_general | solution.py:95
  450.2 26.4 %reduce-scatter.2.cloned.1.call-done = bf16[1,384,512]{2,1,0:T(8,128)(2,1)} async-done(((bf16[1,384,2048]{2,1,0:T(8,128)(2,1)}), bf16[1,384,512]{2,1,0:T(8,128)(2,1)}) %reduce-scatter.2.cloned.1.call-update) | async-done | bytes 393232 | tf_op jit(solution)/shard_map/reduce_scatter | solution.py:101
  476.5 1.9 add_convert_fusion
  (39 shorter events, 0.6 us)
Async XLA Ops:
  6.5 57.3 %copy-start = (bf16[2,128,128]{2,1,0:T(8,128)(2,1)S(1)}, bf16[2,128,128]{2,1,0:T(8,128)(2,1)}, u32[]{:S(2)}) copy-start(bf16[2,128,128]{2,1,0:T(8,128)(2,1)} %param.13) | copy-start | bytes 196612
  6.5 33.1 %all-gather.10.cloned.1.call-start = ((), (), s32[]{:S(2)}) async-start(), calls=%async_computation.2 | async-start | bytes 1310720 | tf_op jit(solution)/shard_map/all_gather | solution.py:30
  7.3 53.0 %all-gather.8.cloned.1.call-start = ((), (), s32[]{:S(2)}) async-start(), calls=%async_computation.1 | async-start | bytes 1966080 | tf_op jit(solution)/shard_map/all_gather | solution.py:35
  18.8 71.0 %all-gather.12.cloned.1.call-start = ((), (), s32[]{:S(2)}) async-start(), calls=%async_computation.3 | async-start | bytes 1310720 | tf_op jit(solution)/shard_map/all_gather | solution.py:69
  19.5 98.3 %all-gather.14.cloned.1.call-start = ((), (), s32[]{:S(2)}) async-start(), calls=%async_computation.4 | async-start | bytes 1966080 | tf_op jit(solution)/shard_map/all_gather | solution.py:81
  63.2 0.9 copy-start.3
  63.8 26.1 %copy-start.1 = (bf16[1,384,512]{2,1,0:T(8,128)(2,1)S(1)}, bf16[1,384,512]{2,1,0:T(8,128)(2,1)}, u32[]{:S(2)}) copy-start(bf16[1,384,512]{2,1,0:T(8,128)(2,1)} %param.10) | copy-start | bytes 1179652
  64.2 33.6 %copy-start.2 = (f32[512]{0:T(512)S(1)}, f32[512]{0:T(512)}, u32[]{:S(2)}) copy-start(f32[512]{0:T(512)} %param.16) | copy-start | bytes 6148
  98.8 127.2 %all-gather.16.cloned.1.call-start = ((), (), s32[]{:S(2)}) async-start(), calls=%async_computation.5 | async-start | bytes 7208960 | tf_op jit(solution)/shard_map/all_gather | solution.py:85
  99.4 233.0 %all-gather.18.cloned.1.call-start = ((), (), s32[]{:S(2)}) async-start(), calls=%async_computation.6 | async-start | bytes 7208960 | tf_op jit(solution)/shard_map/all_gather | solution.py:91
  99.9 338.9 %all-gather.20.cloned.1.call-start = ((), (), s32[]{:S(2)}) async-start(), calls=%async_computation.7 | async-start | bytes 7208960 | tf_op jit(solution)/shard_map/all_gather | solution.py:98
  100.7 375.8 %reduce-scatter.2.cloned.1.call-start = ((), (), s32[]{:S(2)}) async-start(), calls=%async_computation.8 | async-start | bytes 1966080 | tf_op jit(solution)/shard_map/reduce_scatter | solution.py:101
  117.8 321.1 %copy-start.4 = (bf16[1,384,2048]{2,1,0:T(8,128)(2,1)S(1)}, bf16[1,384,2048]{2,1,0:T(8,128)(2,1)}, u32[]{:S(2)}) copy-start(bf16[1,384,2048]{2,1,0:T(8,128)(2,1)} %all-gather.14.cloned.1.call-done) | copy-start | bytes 4718596
Sparse Core Ops, SparseCore 0:
  8.9 30.6 all-gather.9
  41.2 18.9 all-gather.7
  61.8 27.9 all-gather.11
  98.9 18.8 all-gather.13
  119.2 106.6 all-gather.15
  227.4 104.9 all-gather.17
  333.9 104.9 all-gather.19
  450.3 26.2 reduce-scatter.1
where the time goes:
time: 486 us; the launch traced here: 485 us
  waiting for transfers between devices  418 us (86%)
  blocking collectives  23 us (5%)
  matrix products  22.8 us (5%)
  between operations  13.7 us (3%)
  other arithmetic  6.86 us (1%)
    all_gather x1, waiting for transfers between devices, local(): lax.all_gather(gate_weight, 'fs', axis=0, tiled=True)  108 us
    all_gather x1, waiting for transfers between devices, local(): lax.all_gather(down_weight, 'fs', axis=1, tiled=True)  107 us
    all_gather x1, waiting for transfers between devices, local(): lax.all_gather(up_weight, 'fs', axis=0, tiled=True)  99.3 us
    reduce_scatter x1, waiting for transfers between devices, local(): lax.psum_scatter(partial_value.astype(jnp.bfloat16), 'tp', scatter_dimens...  26.4 us
    all_gather x1, waiting for transfers between devices, local(): lax.all_gather(normed, 'tp', axis=2, tiled=True)  20.6 us
    all_gather x1, waiting for transfers between devices, local(): in_full = lax.all_gather(in_weight, 'fs', axis=0, tiled=True)  20 us
    all_gather x1, waiting for transfers between devices, local(): features_full = lax.all_gather(normed_two, 'tp', axis=2, tiled=True)  17 us
    all_gather x1, waiting for transfers between devices, local(): out_full = lax.all_gather(out_weight, 'fs', axis=0, tiled=True)  17 us
  transfers between devices with their start and end apart: 8, of which 8 were waited for; matrix products, arithmetic and copies ran while one was open for 3% of the time, Pallas kernels for 0%

commit v1 on v0

--- a/solution.py
+++ b/solution.py
@@ -7,6 +7,20 @@
 GD = 128
 EPSILON = 0.05
 HALVES = (1, 2, 4, 8)
+
+
+def on_each_block(x, axis, dim, make, out_dim):
+    ways, here, step = (lax.axis_size(axis), lax.axis_index(axis), x.shape[dim])
+    earlier, later = ([], [])
+    going_up = going_down = x
+    for far in range(ways // 2 + 1):
+        earlier.append(make(going_up, (here - far) % ways * step))
+        if 0 < far < ways - ways // 2:
+            later.append(make(going_down, (here + far) % ways * step))
+        going_up = lax.ppermute(going_up, axis, [(d, (d + 1) % ways) for d in range(ways)])
+        going_down = lax.ppermute(going_down, axis, [(d, (d - 1) % ways) for d in range(ways)])
+    line = jnp.concatenate([*earlier[::-1], *later], axis=out_dim)
+    return jnp.roll(line, (here - ways // 2) * earlier[0].shape[out_dim], axis=out_dim)
 
 
 def local(
@@ -92,11 +106,14 @@
         preferred_element_type=jnp.float32,
     )
     hidden = (jax.nn.silu(gate_sum) * up_sum).astype(jnp.bfloat16)
-    partial_value = jnp.einsum(
-        "hor,rn->hon",
-        hidden,
-        lax.all_gather(down_weight, "fs", axis=1, tiled=True),
-        preferred_element_type=jnp.float32,
+    partial_value = on_each_block(
+        down_weight,
+        "fs",
+        1,
+        lambda own_block, at: jnp.einsum(
+            "hor,rn->hon", hidden, own_block, preferred_element_type=jnp.float32
+        ),
+        2,
     )
     summed = lax.psum_scatter(
         partial_value.astype(jnp.bfloat16), "tp", scatter_dimension=2, tiled=True

time: 486 us -> 448 us (0.922)
  waiting for transfers between devices: 418 us -> 359 us
  starting transfers between devices: 0.28 us -> 17.3 us
    all_gather x1 -> x0, waiting for transfers between devices: 107 us -> none  [local(): lax.all_gather(down_weight, 'fs', axis=1, tiled=True)]
    ppermute x0 -> x3, waiting for transfers between devices: none -> 36.7 us  [the longest x2 36.7 us: on_each_block(): lax.ppermute(going_up, axis, [(d, (d + 1) % ways) for d in range(ways)])]
    all_gather x1, waiting for transfers between devices: 108 us -> 136 us  [local(): lax.all_gather(gate_weight, 'fs', axis=0, tiled=True)]
    all_gather x1, waiting for transfers between devices: 17 us -> 0.01 us  [local(): features_full = lax.all_gather(normed_two, 'tp', axis=2, tiled=True)]
    ppermute x0 -> x3, starting transfers between devices: none -> 17 us  [the longest x2 14.4 us: on_each_block(): lax.ppermute(going_up, axis, [(d, (d + 1) % ways) for d in range(ways)])]
    dot_general x1 -> x5, matrix products: 11.3 us -> 14.4 us  [the longest x4 8.58 us: local(): jnp.einsum('hor,rn->hon', hidden, own_block, preferred_element_type=jnp.f...]
  transfers between devices with their start and end apart: 8 -> 10, of which waited for: 8 -> 7; matrix products, arithmetic and copies ran while one was open for 3% -> 6% of each run, Pallas kernels for 0% -> 0%
where the time goes in v1:
time: 448 us
  waiting for transfers between devices  359 us (80%)
  matrix products  26 us (6%)
  blocking collectives  23 us (5%)
  starting transfers between devices  17.3 us (4%)
  between operations  13.8 us (3%)
  other arithmetic  6.85 us (2%)
    all_gather x1, waiting for transfers between devices, local(): lax.all_gather(gate_weight, 'fs', axis=0, tiled=True)  136 us
    all_gather x1, waiting for transfers between devices, local(): lax.all_gather(up_weight, 'fs', axis=0, tiled=True)  99.7 us
    ppermute x2, waiting for transfers between devices, on_each_block(): lax.ppermute(going_up, axis, [(d, (d + 1) % ways) for d in range(ways)])  36.7 us
    reduce_scatter x1, waiting for transfers between devices, local(): lax.psum_scatter(partial_value.astype(jnp.bfloat16), 'tp', scatter_dimens...  26.3 us
    all_gather x1, waiting for transfers between devices, local(): lax.all_gather(normed, 'tp', axis=2, tiled=True)  20.6 us
    all_gather x1, waiting for transfers between devices, local(): in_full = lax.all_gather(in_weight, 'fs', axis=0, tiled=True)  20 us
    all_gather x1, waiting for transfers between devices, local(): out_full = lax.all_gather(out_weight, 'fs', axis=0, tiled=True)  17 us
    ppermute x2, starting transfers between devices, on_each_block(): lax.ppermute(going_up, axis, [(d, (d + 1) % ways) for d in range(ways)])  14.4 us
  transfers between devices with their start and end apart: 10, of which 7 were waited for; matrix products, arithmetic and copies ran while one was open for 6% of the time, Pallas kernels for 0%

profile of v1, /device:TPU:0, one launch (start us, length us, event | category | flops | bytes accessed | tf_op | source)
XLA Modules:
  0.0 447.6 jit_solution(8557717647931341703)
XLA Ops:
  6.5 0.7 all-gather.9.cloned.1.call-update
  7.3 1.2 fusion.16
  8.5 8.4 %psum.14 = f32[1,384]{1,0:T(1,128)S(1)} all-reduce(f32[1,384]{1,0:T(1,128)S(1)} %reduce_sum.23), channel_id=1, replica_groups=mesh['grp'=2,'fs'=4,'tp'=4] {'tp'}, use_global_device_ids=true, to_apply=%region_1.0 | all-reduce | flops 384 | bytes 3072 | tf_op jit(solution)/shard_map/psum | solution.py:40
  16.9 1.9 fusion.18
  18.8 0.7 all-gather.11.cloned.1.call-update
  19.6 20.0 %all-gather.9.cloned.1.call-done = bf16[2048,256]{1,0:T(8,128)(2,1)} async-done(((bf16[512,256]{1,0:T(8,128)(2,1)}), bf16[2048,256]{1,0:T(8,128)(2,1)}) %all-gather.9.cloned.1.call-update) | async-done | bytes 1048592 | tf_op jit(solution)/shard_map/all_gather | solution.py:44
  39.6 20.6 %all-gather.7.cloned.1.call-done = bf16[1,384,2048]{2,1,0:T(8,128)(2,1)} async-done(((bf16[1,384,512]{2,1,0:T(8,128)(2,1)}), bf16[1,384,2048]{2,1,0:T(8,128)(2,1)}) %all-gather.7.cloned.1.call-update) | async-done | bytes 1572880 | tf_op jit(solution)/shard_map/all_gather | solution.py:49
  60.2 2.3 fusion.13
  62.5 0.3 fusion.20
  63.3 0.5 fusion.36
  64.2 8.6 %all_gather.23 = bf16[1,384,1024]{1,2,0:T(8,128)(2,1)S(1)} all-gather(bf16[1,384,256]{1,2,0:T(8,128)(2,1)S(1)} %fusion.35), channel_id=1, replica_groups=mesh['grp'=2,'fs'=4,'tp'=4] {'tp'}, dimensions={2}, use_global_device_ids=true | all-gather | bytes 983040 | tf_op jit(solution)/shard_map/all_gather | solution.py:87
  72.8 17.0 %all-gather.11.cloned.1.call-done = bf16[1024,512]{1,0:T(8,128)(2,1)} async-done(((bf16[256,512]{1,0:T(8,128)(2,1)}), bf16[1024,512]{1,0:T(8,128)(2,1)}) %all-gather.11.cloned.1.call-update) | async-done | bytes 1048592 | tf_op jit(solution)/shard_map/all_gather | solution.py:83
  89.8 1.9 multiply_reduce_fusion
  91.8 6.1 %psum.15 = f32[1,384]{1,0:T(1,128)S(1)} all-reduce(f32[1,384]{1,0:T(1,128)S(1)} %reduce_sum.25), channel_id=1, replica_groups=mesh['grp'=2,'fs'=4,'tp'=4] {'tp'}, use_global_device_ids=true, to_apply=%region_5.6 | all-reduce | flops 384 | bytes 3072 | tf_op jit(solution)/shard_map/psum | solution.py:91
  97.9 0.9 multiply_convert_fusion
  98.8 0.5 all-gather.15.cloned.1.call-update
  99.4 0.5 all-gather.17.cloned.1.call-update
  100.0 1.2 collective-permute-start
  101.2 2.7 collective-permute-start.2
  103.9 36.7 %collective-permute-done = bf16[1408,512]{1,0:T(8,128)(2,1)} collective-permute-done((bf16[1408,512]{1,0:T(8,128)(2,1)}, bf16[1408,512]{1,0:T(8,128)(2,1)}, u32[]{:S(2)}, u32[]{:S(2)}) %collective-permute-start) | collective-permute-done | bytes 1441824 | tf_op jit(solution)/shard_map/ppermute | solution.py:20
  140.6 13.2 %collective-permute-start.1 = (bf16[1408,512]{1,0:T(8,128)(2,1)}, bf16[1408,512]{1,0:T(8,128)(2,1)}, u32[]{:S(2)}, u32[]{:S(2)}) collective-permute-start(bf16[1408,512]{1,0:T(8,128)(2,1)} %collective-permute-done), channel_id=1, source_target_pairs={{0,4},{4,8},{8,12},{12,0},{1,5},{5,9},{9,13},{13,1},{2,6},{6,10},{... | collective-permute-start | bytes 4325384 | tf_op jit(solution)/shard_map/ppermute | solution.py:20
  153.8 135.8 %all-gather.15.cloned.1.call-done = bf16[2048,1408]{1,0:T(8,128)(2,1)} async-done(((bf16[512,1408]{1,0:T(8,128)(2,1)}), bf16[2048,1408]{1,0:T(8,128)(2,1)}) %all-gather.15.cloned.1.call-update) | async-done | bytes 5767184 | tf_op jit(solution)/shard_map/all_gather | solution.py:99
  289.6 7.2 %fusion.2 = f32[384,1408]{1,0:T(8,128)} fusion(bf16[2048,1408]{1,0:T(8,128)(2,1)} %all-gather.15.cloned.1.call-done, bf16[1,384,2048]{2,1,0:T(8,128)(2,1)} %all-gather.13.cloned.1.call-done), kind=kOutput, calls=%fused_computation.4 | convolution fusion | flops 2214592512 | bytes 9502720 | tf_op jit(solution)/shard_map/slk,kf->slf/dot_general | solution.py:96
  296.8 99.7 %all-gather.17.cloned.1.call-done = bf16[2048,1408]{1,0:T(8,128)(2,1)} async-done(((bf16[512,1408]{1,0:T(8,128)(2,1)}), bf16[2048,1408]{1,0:T(8,128)(2,1)}) %all-gather.17.cloned.1.call-update) | async-done | bytes 5767184 | tf_op jit(solution)/shard_map/all_gather | solution.py:105
  396.5 5.8 %fusion = bf16[384,1408]{1,0:T(8,128)(2,1)S(1)} fusion(bf16[2048,1408]{1,0:T(8,128)(2,1)} %all-gather.17.cloned.1.call-done, f32[384,1408]{1,0:T(8,128)} %fusion.2, bf16[1,384,2048]{2,1,0:T(8,128)(2,1)S(1)} %copy-done.4), kind=kOutput, calls=%fused_computation.2 | convolution fusion | flops 2217836544 | bytes 10584064 | tf_op jit(solution)/shard_map/slk,kf->slf/dot_general | solution.py:102
  402.4 2.1 constant_dynamic-update-slice_fusion.7
  404.5 2.1 constant_dynamic-update-slice_fusion.6
  406.7 2.1 constant_dynamic-update-slice_fusion.5
  408.8 2.1 constant_dynamic-update-slice_fusion.4
  411.2 1.4 dynamic-slice_convert_fusion
  412.6 26.3 %reduce-scatter.2.cloned.1.call-done = bf16[1,384,512]{2,1,0:T(8,128)(2,1)} async-done(((bf16[1,384,2048]{2,1,0:T(8,128)(2,1)}), bf16[1,384,512]{2,1,0:T(8,128)(2,1)}) %reduce-scatter.2.cloned.1.call-update) | async-done | bytes 393232 | tf_op jit(solution)/shard_map/reduce_scatter | solution.py:118
  438.9 1.9 add_convert_fusion
  (51 shorter events, 1.4 us)
Async XLA Ops:
  6.5 57.3 %copy-start = (bf16[2,128,128]{2,1,0:T(8,128)(2,1)S(1)}, bf16[2,128,128]{2,1,0:T(8,128)(2,1)}, u32[]{:S(2)}) copy-start(bf16[2,128,128]{2,1,0:T(8,128)(2,1)} %param.13) | copy-start | bytes 196612
  6.5 33.1 %all-gather.9.cloned.1.call-start = ((), (), s32[]{:S(2)}) async-start(), calls=%async_computation.2 | async-start | bytes 1310720 | tf_op jit(solution)/shard_map/all_gather | solution.py:44
  7.3 53.0 %all-gather.7.cloned.1.call-start = ((), (), s32[]{:S(2)}) async-start(), calls=%async_computation.1 | async-start | bytes 1966080 | tf_op jit(solution)/shard_map/all_gather | solution.py:49
  18.8 71.0 %all-gather.11.cloned.1.call-start = ((), (), s32[]{:S(2)}) async-start(), calls=%async_computation.3 | async-start | bytes 1310720 | tf_op jit(solution)/shard_map/all_gather | solution.py:83
  19.5 134.2 %all-gather.13.cloned.1.call-start = ((), (), s32[]{:S(2)}) async-start(), calls=%async_computation.4 | async-start | bytes 1966080 | tf_op jit(solution)/shard_map/all_gather | solution.py:95
  63.2 0.9 copy-start.3
  63.8 26.1 %copy-start.1 = (bf16[1,384,512]{2,1,0:T(8,128)(2,1)S(1)}, bf16[1,384,512]{2,1,0:T(8,128)(2,1)}, u32[]{:S(2)}) copy-start(bf16[1,384,512]{2,1,0:T(8,128)(2,1)} %param.10) | copy-start | bytes 1179652
  72.8 25.1 %copy-start.2 = (f32[512]{0:T(512)S(1)}, f32[512]{0:T(512)}, u32[]{:S(2)}) copy-start(f32[512]{0:T(512)} %param.16) | copy-start | bytes 6148
  98.8 190.8 %all-gather.15.cloned.1.call-start = ((), (), s32[]{:S(2)}) async-start(), calls=%async_computation.5 | async-start | bytes 7208960 | tf_op jit(solution)/shard_map/all_gather | solution.py:99
  99.4 297.1 %all-gather.17.cloned.1.call-start = ((), (), s32[]{:S(2)}) async-start(), calls=%async_computation.6 | async-start | bytes 7208960 | tf_op jit(solution)/shard_map/all_gather | solution.py:105
  99.9 338.9 %reduce-scatter.2.cloned.1.call-start = ((), (), s32[]{:S(2)}) async-start(), calls=%async_computation.7 | async-start | bytes 1966080 | tf_op jit(solution)/shard_map/reduce_scatter | solution.py:118
  100.0 40.6 %collective-permute-start = (bf16[1408,512]{1,0:T(8,128)(2,1)}, bf16[1408,512]{1,0:T(8,128)(2,1)}, u32[]{:S(2)}, u32[]{:S(2)}) collective-permute-start(bf16[1408,512]{1,0:T(8,128)(2,1)} %param.19), channel_id=1, source_target_pairs={{0,4},{4,8},{8,12},{12,0},{1,5},{5,9},{9,13},{13,1},{2,6},{6,10},{... | collective-permute-start | bytes 4325384 | tf_op jit(solution)/shard_map/ppermute | solution.py:20
  101.2 307.6 %collective-permute-start.2 = (bf16[1408,512]{1,0:T(8,128)(2,1)}, bf16[1408,512]{1,0:T(8,128)(2,1)}, u32[]{:S(2)}, u32[]{:S(2)}) collective-permute-start(bf16[1408,512]{1,0:T(8,128)(2,1)} %param.19), channel_id=1, source_target_pairs={{0,12},{4,0},{8,4},{12,8},{1,13},{5,1},{9,5},{13,9},{2,14},{6,2},{... | collective-permute-start | bytes 4325384 | tf_op jit(solution)/shard_map/ppermute | solution.py:21
  140.6 261.7 %collective-permute-start.1 = (bf16[1408,512]{1,0:T(8,128)(2,1)}, bf16[1408,512]{1,0:T(8,128)(2,1)}, u32[]{:S(2)}, u32[]{:S(2)}) collective-permute-start(bf16[1408,512]{1,0:T(8,128)(2,1)} %collective-permute-done), channel_id=1, source_target_pairs={{0,4},{4,8},{8,12},{12,0},{1,5},{5,9},{9,13},{13,1},{2,6},{6,10},{... | collective-permute-start | bytes 4325384 | tf_op jit(solution)/shard_map/ppermute | solution.py:20
  153.8 242.7 %copy-start.4 = (bf16[1,384,2048]{2,1,0:T(8,128)(2,1)S(1)}, bf16[1,384,2048]{2,1,0:T(8,128)(2,1)}, u32[]{:S(2)}) copy-start(bf16[1,384,2048]{2,1,0:T(8,128)(2,1)} %all-gather.13.cloned.1.call-done) | copy-start | bytes 4718596
Sparse Core Ops, SparseCore 0:
  8.9 30.6 all-gather.8
  41.2 18.9 all-gather.6
  61.8 27.9 all-gather.10
  98.9 18.8 all-gather.12
  119.2 170.3 all-gather.14
  291.1 105.3 all-gather.16
  412.7 26.1 reduce-scatter.1
